TPU v7x, 32 devices: a whole 2x2x4 slice. The times are simulated.
32 devices in a mesh: sp: 8 (over z, y), dp: 4 (over x, core).
Axes of the slice: x: 2, y: 2, z: 4, core: 2. Of those that a mesh axis runs over, the one named last changes fastest.
Arguments:
- layer_input: bfloat16 [4, 1024, 2048], P('dp', 'sp'), may hold values from -0.0390625 to 0.0390625
- queries: bfloat16 [4, 1024, 2048], P('dp', 'sp'), may hold values from -6 to 6
- key_vectors: bfloat16 [4, 1024, 2048], P('dp', 'sp'), may hold values from -6 to 6
- values: bfloat16 [4, 1024, 4096], P('dp', 'sp'), may hold values from -6 to 6
- cotangent: bfloat16 [4, 1024, 4096], P('dp', 'sp'), may hold values from -0.3125 to 0.3125
- log_decay: float32 [4, 16, 1024], P('dp', 'sp'), may hold values from -3 to 0
- key_weight: bfloat16 [2048, 2048], P('dp'), may hold values from -0.125 to 0.125
Outputs:
- grad_query: bfloat16 [4, 1024, 2048], P('dp', 'sp')
- grad_value: bfloat16 [4, 1024, 4096], P('dp', 'sp')
- grad_input: bfloat16 [4, 1024, 2048], P('dp', 'sp')
- grad_key_weight: float32 [2048, 2048], P('dp')
All inputs are finite; a program needn't handle non-finite values.
Results may differ from a plain program's by a relative error of at most 0.012.
Values may be sent and summed in bfloat16 or wider, within the bound.
A program may use at most 128 MiB of HBM per device.

v0:
```python
import functools

import jax
import jax.numpy as jnp
from jax import lax
from jax.experimental import pallas as pl
from jax.experimental.pallas import tpu as pltpu
from jax.sharding import PartitionSpec as P

HEADS = 8
BLOCK = 128
MESH = pl.DeviceIdType.MESH
BF16 = jnp.bfloat16
F32 = jnp.float32


def dot_nn(a, b):
    return lax.dot_general(a, b, (((1,), (0,)), ((), ())), preferred_element_type=F32)


def dot_nt(a, b):
    return lax.dot_general(a, b, (((1,), (1,)), ((), ())), preferred_element_type=F32)


def dot_tn(a, b):
    return lax.dot_general(a, b, (((0,), (0,)), ((), ())), preferred_element_type=F32)


def decay_columns(lam_ref, b):
    lam_fwd = lam_ref[0, b]
    lam_bwd = lam_ref[1, b]
    row = lax.broadcasted_iota(jnp.int32, (BLOCK, BLOCK), 0)
    col = lax.broadcasted_iota(jnp.int32, (BLOCK, BLOCK), 1)
    lower = col <= row
    c0 = jnp.sum(jnp.where(lower, lam_fwd, 0.0), axis=1, keepdims=True)
    c1 = jnp.sum(jnp.where(col >= row, lam_bwd, 0.0), axis=1, keepdims=True)
    e0 = jnp.sum(lam_fwd, axis=1, keepdims=True)
    e1 = jnp.sum(lam_bwd, axis=1, keepdims=True)
    return c0, c1, e0, e1, row, col, lower


def as_row(column, row, col):
    return jnp.sum(jnp.where(row == col, column, 0.0), axis=0, keepdims=True)


def retention_kernel(
    sp,
    q_in, k_in, v_in, g_in, lam_ref,
    q_home, k_home, v_home, k_head,
    qa, ka, va, ga,
    qacc, kacc, vacc,
    dm0, dm1, dg0, dg1,
    sm0, sg1,
    run_a, run_b,
    qh, kh, vh,
    in_send, in_recv, out_send, out_recv, local_sem, head_sem,
):
    me = lax.axis_index("sp")
    dk = qa.shape[1]
    dv = va.shape[1]
    scaling = dk ** (-0.5)
    ins = ((q_in, qa, dk), (k_in, ka, dk), (v_in, va, dv), (g_in, ga, dv))
    outs = ((qh, q_home, dk), (kh, k_home, dk), (vh, v_home, dv))

    def rows_of(b):
        return pl.ds(pl.multiple_of(b * BLOCK, BLOCK), BLOCK)

    def cols_of(b, width):
        return pl.ds(pl.multiple_of(b * width, width), width)

    locals_in = [
        pltpu.make_async_copy(src.at[:, cols_of(me, w)], dst.at[rows_of(me)], local_sem.at[t])
        for t, (src, dst, w) in enumerate(ins)
    ]
    for copy in locals_in:
        copy.start()

    barrier = pltpu.get_barrier_semaphore()
    for off in range(1, sp):
        pl.semaphore_signal(
            barrier, inc=1, device_id={"sp": lax.rem(me + off, sp)}, device_id_type=MESH
        )
    pl.semaphore_wait(barrier, sp - 1)

    def incoming(t, off):
        src, dst, w = ins[t]
        peer = lax.rem(me + off, sp)
        return pltpu.make_async_remote_copy(
            src_ref=src.at[:, cols_of(peer, w)],
            dst_ref=dst.at[rows_of(me)],
            send_sem=in_send.at[t, off],
            recv_sem=in_recv.at[t, off],
            device_id={"sp": peer},
            device_id_type=MESH,
        )

    for off in range(1, sp):
        for t in range(4):
            incoming(t, off).start()

    def local_part(b):
        rows = rows_of(b)
        q, k, v, g = qa[rows, :], ka[rows, :], va[rows, :], ga[rows, :]
        c0, c1, e0, e1, row, col, lower = decay_columns(lam_ref, b)
        spread = jnp.where(lower, c0 - as_row(c0, row, col), c1 - as_row(c1, row, col))
        weights = jnp.exp(spread) * scaling
        scores = (dot_nt(q, k) * weights).astype(BF16)
        grads = (dot_nt(g, v) * weights).astype(BF16)
        qacc[rows, :] = dot_nn(grads, k)
        kacc[rows, :] = dot_tn(grads, q)
        vacc[rows, :] = dot_tn(scores, g)
        qf, kf = q.astype(F32), k.astype(F32)
        dm0[b] = dot_tn((kf * jnp.exp(e0 - c0)).astype(BF16), v)
        dm1[b] = dot_tn((kf * jnp.exp(e1 - c1)).astype(BF16), v)
        dg0[b] = dot_tn((qf * (jnp.exp(c0) * scaling)).astype(BF16), g)
        dg1[b] = dot_tn((qf * (jnp.exp(c1) * scaling)).astype(BF16), g)

    for copy in locals_in:
        copy.wait()
    local_part(me)

    def arrive(off, carry):
        for t in range(4):
            incoming(t, off).wait_recv()
        local_part(lax.rem(me + sp - off, sp))
        return carry

    lax.fori_loop(1, sp, arrive, 0)

    run_a[...] = jnp.zeros_like(run_a)
    run_b[...] = jnp.zeros_like(run_b)

    def forward(b, carry):
        e0 = jnp.exp(jnp.sum(lam_ref[0, b], axis=1, keepdims=True))
        e1 = jnp.exp(jnp.sum(lam_ref[1, b], axis=1, keepdims=True))
        m0 = run_a[...]
        sm0[b] = m0.astype(BF16)
        run_a[...] = e0 * m0 + dm0[b]
        g1 = run_b[...]
        sg1[b] = g1.astype(BF16)
        run_b[...] = e1 * g1 + dg1[b]
        return carry

    lax.fori_loop(0, sp, forward, 0)

    run_a[...] = jnp.zeros_like(run_a)
    run_b[...] = jnp.zeros_like(run_b)

    def outgoing(t, b, source):
        src, dst, w = outs[t]
        return pltpu.make_async_remote_copy(
            src_ref=src.at[rows_of(b)],
            dst_ref=dst.at[:, cols_of(source, w)],
            send_sem=out_send.at[t, b],
            recv_sem=out_recv.at[t, source],
            device_id={"sp": b},
            device_id_type=MESH,
        )

    def local_out(t):
        src, dst, w = outs[t]
        return pltpu.make_async_copy(src.at[rows_of(me)], dst.at[:, cols_of(me, w)], local_sem.at[t])

    def backward(step, carry):
        b = sp - 1 - step
        rows = rows_of(b)
        k, v, g = ka[rows, :], va[rows, :], ga[rows, :]
        c0, c1, e0, e1, _, _, _ = decay_columns(lam_ref, b)
        kf = k.astype(F32)
        ks0, ks1 = jnp.exp(e0 - c0), jnp.exp(e1 - c1)
        m0, g1 = sm0[b], sg1[b]
        g0, m1 = run_a[...].astype(BF16), run_b[...].astype(BF16)
        qh[rows, :] = (
            qacc[rows, :]
            + dot_nt(g, m0) * (jnp.exp(c0) * scaling)
            + dot_nt(g, m1) * (jnp.exp(c1) * scaling)
        ).astype(BF16)
        kh[rows, :] = (kacc[rows, :] + dot_nt(v, g0) * ks0 + dot_nt(v, g1) * ks1).astype(BF16)
        vh[rows, :] = (
            vacc[rows, :]
            + dot_nn((kf * ks0).astype(BF16), g0)
            + dot_nn((kf * ks1).astype(BF16), g1)
        ).astype(BF16)
        run_a[...] = jnp.exp(e0) * run_a[...] + dg0[b]
        run_b[...] = jnp.exp(e1) * run_b[...] + dm1[b]

        @pl.when(b != me)
        def _():
            for t in (1, 0, 2):
                outgoing(t, b, me).start()

        @pl.when(b == me)
        def _():
            for t in range(3):
                local_out(t).start()

        return carry

    lax.fori_loop(0, sp, backward, 0)

    head_copy = pltpu.make_async_copy(kh, k_head, head_sem)
    head_copy.start()

    for t in range(3):
        local_out(t).wait()

    for off in range(1, sp):
        for t in range(4):
            incoming(t, off).wait_send()

    def settle(off, carry):
        peer = lax.rem(me + off, sp)
        for t in range(3):
            outgoing(t, peer, peer).wait()
        return carry

    lax.fori_loop(1, sp, settle, 0)
    head_copy.wait()


def retention_by_head(queries, key_vectors, values, cotangent, log_decay, sp):
    tokens, hk = queries.shape
    hv = values.shape[1]
    length = tokens * sp
    dk, dv = hk // HEADS, hv // HEADS
    lam = log_decay.reshape(2, sp, 1, BLOCK)
    anyspace = pl.BlockSpec(memory_space=pl.ANY)
    return pl.pallas_call(
        functools.partial(retention_kernel, sp),
        out_shape=(
            jax.ShapeDtypeStruct((tokens, hk), BF16),
            jax.ShapeDtypeStruct((tokens, hk), BF16),
            jax.ShapeDtypeStruct((tokens, hv), BF16),
            jax.ShapeDtypeStruct((length, dk), BF16),
        ),
        in_specs=[anyspace] * 4 + [pl.BlockSpec(memory_space=pltpu.VMEM)],
        out_specs=(anyspace,) * 4,
        scratch_shapes=[
            pltpu.VMEM((length, dk), BF16),
            pltpu.VMEM((length, dk), BF16),
            pltpu.VMEM((length, dv), BF16),
            pltpu.VMEM((length, dv), BF16),
            pltpu.VMEM((length, dk), F32),
            pltpu.VMEM((length, dk), F32),
            pltpu.VMEM((length, dv), F32),
            pltpu.VMEM((sp, dk, dv), F32),
            pltpu.VMEM((sp, dk, dv), F32),
            pltpu.VMEM((sp, dk, dv), F32),
            pltpu.VMEM((sp, dk, dv), F32),
            pltpu.VMEM((sp, dk, dv), BF16),
            pltpu.VMEM((sp, dk, dv), BF16),
            pltpu.VMEM((dk, dv), F32),
            pltpu.VMEM((dk, dv), F32),
            pltpu.VMEM((length, dk), BF16),
            pltpu.VMEM((length, dk), BF16),
            pltpu.VMEM((length, dv), BF16),
            pltpu.SemaphoreType.DMA((4, sp)),
            pltpu.SemaphoreType.DMA((4, sp)),
            pltpu.SemaphoreType.DMA((3, sp)),
            pltpu.SemaphoreType.DMA((3, sp)),
            pltpu.SemaphoreType.DMA((4,)),
            pltpu.SemaphoreType.DMA(()),
        ],
        compiler_params=pltpu.CompilerParams(
            collective_id=0, has_side_effects=True, vmem_limit_bytes=50 * 1024 * 1024
        ),
        cost_estimate=pl.CostEstimate(
            flops=6_000_000_000, bytes_accessed=150_000_000, transcendentals=0
        ),
    )(queries, key_vectors, values, cotangent, lam)


def shards_by_head(sp, layer_input, queries, key_vectors, values, cotangent, log_decay, key_weight):
    all_weight = lax.all_gather(key_weight, "dp", axis=0, tiled=True)
    all_rows = lax.all_gather(layer_input[0], "sp", axis=0, tiled=True)
    grad_query, grad_key, grad_value, key_head = retention_by_head(
        queries[0], key_vectors[0], values[0], cotangent[0], log_decay[0], sp
    )
    partial = lax.dot_general(
        all_rows, key_head, (((0,), (0,)), ((), ())), preferred_element_type=F32
    ).astype(BF16)
    summed = lax.psum_scatter(partial, "dp", scatter_dimension=0, tiled=True)
    grad_input = lax.dot_general(
        grad_key, all_weight, (((1,), (1,)), ((), ())), preferred_element_type=F32
    ).astype(BF16)
    grad_weight = lax.all_gather(summed, "sp", axis=1, tiled=True).astype(F32)
    return (grad_query[None], grad_value[None], grad_input[None], grad_weight)


def unit_backward(query_rows, key_rows, value_rows, grad_rows, decay_rows, strict):
    length, key_width = query_rows.shape
    value_width = value_rows.shape[1]
    blocks = length // BLOCK
    scaling = key_width ** (-0.5)
    query_blk = query_rows.reshape(blocks, BLOCK, key_width)
    key_blk = key_rows.reshape(blocks, BLOCK, key_width)
    value_blk = value_rows.reshape(blocks, BLOCK, value_width)
    grad_blk = grad_rows.reshape(blocks, BLOCK, value_width)
    within = jnp.cumsum(decay_rows.reshape(blocks, BLOCK), axis=1)
    position_slots = jnp.arange(BLOCK)
    allowed = jnp.where(
        strict,
        position_slots[None, :] < position_slots[:, None],
        position_slots[None, :] <= position_slots[:, None],
    )
    spread = jnp.where(allowed, within[:, :, None] - within[:, None, :], 0.0)
    weights = jnp.where(allowed, jnp.exp(spread), 0.0) * scaling
    raw_scores = jnp.einsum("nid,njd->nij", query_blk, key_blk, preferred_element_type=jnp.float32)
    scores = (raw_scores * weights).astype(jnp.bfloat16)
    raw_grads = jnp.einsum("niv,njv->nij", grad_blk, value_blk, preferred_element_type=jnp.float32)
    grad_scores = (raw_grads * weights).astype(jnp.bfloat16)
    value_inner = jnp.einsum("nij,niv->njv", scores, grad_blk, preferred_element_type=jnp.float32)
    query_inner = jnp.einsum(
        "nij,njd->nid", grad_scores, key_blk, preferred_element_type=jnp.float32
    )
    key_inner = jnp.einsum(
        "nij,nid->njd", grad_scores, query_blk, preferred_element_type=jnp.float32
    )
    ending = within[:, -1:]
    query_scale = jnp.exp(within) * scaling
    key_scale = jnp.exp(ending - within)
    carry_decay = jnp.exp(ending[:, 0])
    query_dec = (query_blk * query_scale[:, :, None]).astype(jnp.bfloat16)
    key_dec = (key_blk * key_scale[:, :, None]).astype(jnp.bfloat16)
    contract = (((0,), (0,)), ((), ()))

    def advance(memory, inputs):
        key_b, value_b, factor = inputs
        before = memory.astype(jnp.bfloat16)
        memory = factor * memory + lax.dot_general(
            key_b, value_b, contract, preferred_element_type=jnp.float32
        )
        return (memory, before)

    start_state = jnp.zeros((key_width, value_width), jnp.float32)
    _, states_before = lax.scan(advance, start_state, (key_dec, value_blk, carry_decay))

    def retreat(later, inputs):
        query_b, grad_b, factor = inputs
        after = later.astype(jnp.bfloat16)
        later = factor * later + lax.dot_general(
            query_b, grad_b, contract, preferred_element_type=jnp.float32
        )
        return (later, after)

    _, state_grads = lax.scan(
        retreat, start_state, (query_dec, grad_blk, carry_decay), reverse=True
    )
    query_carried = jnp.einsum(
        "niv,ndv->nid", grad_blk, states_before, preferred_element_type=jnp.float32
    )
    key_carried = jnp.einsum(
        "njv,ndv->njd", value_blk, state_grads, preferred_element_type=jnp.float32
    )
    value_carried = jnp.einsum(
        "njd,ndv->njv", key_dec, state_grads, preferred_element_type=jnp.float32
    )
    grad_q = query_inner + query_carried * query_scale[:, :, None]
    grad_k = key_inner + key_carried * key_scale[:, :, None]
    grad_v = value_inner + value_carried
    return (
        grad_q.reshape(length, key_width),
        grad_k.reshape(length, key_width),
        grad_v.reshape(length, value_width),
    )


def unit_grads(query_rows, key_rows, value_rows, grad_rows, decay_rows, backward):

    def orient(array):
        return jnp.where(backward, jnp.flip(array, 0), array)

    gradients = unit_backward(
        orient(query_rows),
        orient(key_rows),
        orient(value_rows),
        orient(grad_rows),
        orient(decay_rows),
        backward,
    )
    return tuple((orient(single).astype(jnp.bfloat16) for single in gradients))


def shards_by_unit(layer_input, queries, key_vectors, values, cotangent, log_decay, key_weight):
    tokens = layer_input.shape[1]
    key_width = queries.shape[2] // HEADS
    value_width = values.shape[2] // HEADS

    def to_units(array, head_width):
        shaped = array[0].reshape(tokens, HEADS, head_width)
        return jnp.moveaxis(jnp.repeat(shaped, 2, axis=1), 1, 0)

    sent = (
        to_units(queries, key_width),
        to_units(key_vectors, key_width),
        to_units(values, value_width),
        to_units(cotangent, value_width),
    )
    query_units, key_units, value_units, grad_units = (
        lax.all_to_all(sent[0], "sp", split_axis=0, concat_axis=1, tiled=True),
        lax.all_to_all(sent[1], "sp", split_axis=0, concat_axis=1, tiled=True),
        lax.all_to_all(sent[2], "sp", split_axis=0, concat_axis=1, tiled=True),
        lax.all_to_all(sent[3], "sp", split_axis=0, concat_axis=1, tiled=True),
    )
    local_units = query_units.shape[0]
    first_unit = lax.axis_index("sp") * local_units
    backward = (first_unit + jnp.arange(local_units)) % 2 == 1
    query_back, key_back, value_back = jax.vmap(unit_grads)(
        query_units, key_units, value_units, grad_units, log_decay[0], backward
    )
    query_home, key_home, value_home = (
        lax.all_to_all(query_back, "sp", split_axis=1, concat_axis=0, tiled=True),
        lax.all_to_all(key_back, "sp", split_axis=1, concat_axis=0, tiled=True),
        lax.all_to_all(value_back, "sp", split_axis=1, concat_axis=0, tiled=True),
    )

    def merge_dirs(array, head_width):
        paired = array.astype(jnp.float32).reshape(HEADS, 2, tokens, head_width).sum(axis=1)
        return jnp.moveaxis(paired, 0, 1).reshape(tokens, HEADS * head_width).astype(jnp.bfloat16)

    grad_query = merge_dirs(query_home, key_width)
    grad_key = merge_dirs(key_home, key_width)
    grad_value = merge_dirs(value_home, value_width)
    grad_input = lax.dot_general(
        grad_key,
        lax.all_gather(key_weight, "dp", axis=0, tiled=True),
        (((1,), (1,)), ((), ())),
        preferred_element_type=jnp.float32,
    ).astype(jnp.bfloat16)
    token_rows = layer_input[0]
    summed = lax.psum_scatter(
        lax.dot_general(
            token_rows, grad_key, (((0,), (0,)), ((), ())), preferred_element_type=jnp.float32
        ),
        "dp",
        scatter_dimension=0,
        tiled=True,
    )
    grad_weight = lax.psum(summed, "sp")
    return (grad_query[None], grad_value[None], grad_input[None], grad_weight)


def shards(*arrays):
    sp = lax.axis_size("sp")
    if sp == HEADS and arrays[1].shape[1] == BLOCK:
        return shards_by_head(sp, *arrays)
    return shards_by_unit(*arrays)


def solution(mesh):
    return jax.shard_map(
        shards,
        mesh=mesh,
        in_specs=(
            P("dp", "sp", None),
            P("dp", "sp", None),
            P("dp", "sp", None),
            P("dp", "sp", None),
            P("dp", "sp", None),
            P("dp", "sp", None),
            P("dp", None),
        ),
        out_specs=(P("dp", "sp", None), P("dp", "sp", None), P("dp", "sp", None), P("dp", None)),
        check_vma=False,
    )
```

profile of v0, /device:TPU:15, one launch (start us, length us, event | category | flops | bytes accessed | tf_op | source)
XLA Modules:
  0.0 346.9 jit_solution(3785313645634679863)
XLA Ops:
  7.2 0.0 all-gather.9.cloned.1.call-start
  7.2 0.7 all-gather.9.cloned.1.call-update
  7.9 0.0 reduce-scatter.2.cloned.1.call-start
  7.9 0.7 reshape_squeeze.3.lam_ref
  8.7 0.0 copy-start
  8.7 1.0 copy-done
  9.7 0.0 copy-start.1
  9.7 1.0 copy-done.1
  10.8 167.5 %shard_map.102 = (bf16[128,2048]{1,0:T(8,128)(2,1)S(1)}, bf16[128,2048]{1,0:T(8,128)(2,1)S(1)}, bf16[128,4096]{1,0:T(8,128)(2,1)S(1)}, bf16[1024,256]{1,0:T(8,128)(2,1)S(1)}) custom-call(bf16[128,2048]{1,0:T(8,128)(2,1)S(1)} %bitcast.22, bf16[128,2048]{1,0:T(8,128)(2,1)S(1)} %bitcast.23, bf16[128,4096]{1,0:T(8,128)(2,1)} %bitcast.24, ...), custom_call_target="tpu_custom_call" | custom-call | flops 6000000000 | bytes 150000000 | tf_op jit(solution)/shard_map/pallas_call | solution.py:228
  178.3 0.0 all-gather.9.cloned.1.call-done
  178.3 4.4 %fusion.5 = bf16[2048,256]{0,1:T(8,128)(2,1)} fusion(bf16[1024,256]{1,0:T(8,128)(2,1)S(1)} %get-tuple-element.11, bf16[1,1024,2048]{2,1,0:T(8,128)(2,1)} %all-gather.9.cloned.1.call-done), kind=kOutput, calls=%fused_computation.3 | convolution fusion | flops 1074266112 | bytes 5767168 | tf_op jit(solution)/shard_map/dot_general | solution.py:279
  182.8 0.0 reduce-scatter.2.cloned.1.call-update
  182.8 0.0 all-gather.5.cloned.1.call-start
  182.8 0.7 all-gather.5.cloned.1.call-update
  183.5 0.0 all-gather.7.cloned.1.call-start
  183.6 40.8 %reduce-scatter.2.cloned.1.call-done = bf16[512,256]{0,1:T(8,128)(2,1)} async-done(((bf16[2048,256]{0,1:T(8,128)(2,1)}), bf16[512,256]{0,1:T(8,128)(2,1)}) %reduce-scatter.2.cloned.1.call-update) | async-done | bytes 262160 | tf_op jit(solution)/shard_map/reduce_scatter | solution.py:282
  224.4 0.0 all-gather.7.cloned.1.call-update
  224.4 60.4 %all-gather.5.cloned.1.call-done = bf16[2048,2048]{1,0:T(8,128)(2,1)} async-done(((bf16[512,2048]{1,0:T(8,128)(2,1)}), bf16[2048,2048]{1,0:T(8,128)(2,1)}) %all-gather.5.cloned.1.call-update) | async-done | bytes 8388624 | tf_op jit(solution)/shard_map/all_gather | solution.py:274
  284.9 7.1 %fusion.8 = bf16[1,128,2048]{2,1,0:T(8,128)(2,1)} fusion(bf16[128,2048]{1,0:T(8,128)(2,1)S(1)} %get-tuple-element.10, bf16[2048,2048]{1,0:T(8,128)(2,1)} %all-gather.5.cloned.1.call-done), kind=kOutput, calls=%fused_computation.5 | convolution fusion | flops 1074003968 | bytes 9437184 | tf_op jit(solution)/shard_map/dot_general | solution.py:283
  291.9 42.6 %all-gather.7.cloned.1.call-done = bf16[512,2048]{0,1:T(8,128)(2,1)} async-done(((bf16[512,256]{0,1:T(8,128)(2,1)}), bf16[512,2048]{0,1:T(8,128)(2,1)}) %all-gather.7.cloned.1.call-update) | async-done | bytes 2097168 | tf_op jit(solution)/shard_map/all_gather | solution.py:286
  334.5 4.1 %copy.11 = f32[512,2048]{1,0:T(8,128)} copy(bf16[512,2048]{0,1:T(8,128)(2,1)} %all-gather.7.cloned.1.call-done) | data formatting | bytes 6291456
  338.6 0.8 copy.14
  339.4 1.0 copy.15
Async XLA Ops:
  7.2 171.2 %all-gather.9.cloned.1.call-start = ((), (), s32[]{:S(2)}) async-start(), calls=%async_computation.4 | async-start | bytes 4718592 | tf_op jit(solution)/shard_map/all_gather | solution.py:275
  7.9 216.5 %reduce-scatter.2.cloned.1.call-start = ((), (), s32[]{:S(2)}) async-start(), calls=%async_computation.2 | async-start | bytes 1310720 | tf_op jit(solution)/shard_map/reduce_scatter | solution.py:282
  8.7 1.0 copy-start
  9.7 1.0 copy-start.1
  182.8 102.1 %all-gather.5.cloned.1.call-start = ((), (), s32[]{:S(2)}) async-start(), calls=%async_computation.1 | async-start | bytes 10485760 | tf_op jit(solution)/shard_map/all_gather | solution.py:274
  183.5 151.0 %all-gather.7.cloned.1.call-start = ((), (), s32[]{:S(2)}) async-start(), calls=%async_computation.3 | async-start | bytes 2359296 | tf_op jit(solution)/shard_map/all_gather | solution.py:286
Sparse Core Ops, SparseCore 0:
  10.1 145.0 all-gather.8
  182.9 41.4 reduce-scatter.1
  226.0 58.8 all-gather.4
  286.8 47.6 all-gather.6
where the time goes:
time: 351 us; the launch traced here: 347 us
  Pallas kernels  168 us (48%)
  waiting for transfers between devices  145 us (41%)
  between operations  13.8 us (4%)
  matrix products  11.5 us (3%)
  local copies, waits for them, and re-layouts  8.64 us (2%)
    pallas_call x1, Pallas kernels, retention_by_head(): pl.pallas_call(functools.partial(retention_kernel, sp), out_shape=(jax.Sh...  168 us
    all_gather x1, waiting for transfers between devices, shards_by_head(): all_weight = lax.all_gather(key_weight, 'dp', axis=0, tiled=True)  60.4 us
    all_gather x1, waiting for transfers between devices, shards_by_head(): grad_weight = lax.all_gather(summed, 'sp', axis=1, tiled=True).astype(F32)  42.6 us
    reduce_scatter x1, waiting for transfers between devices, shards_by_head(): summed = lax.psum_scatter(partial, 'dp', scatter_dimension=0, tiled=True)  40.8 us
    unnamed x7, local copies, waits for them, and re-layouts  7.92 us
    dot_general x1, matrix products, shards_by_head(): lax.dot_general(grad_key, all_weight, (((1,), (1,)), ((), ())), preferred...  7.06 us
  transfers between devices with their start and end apart: 4, of which 3 were waited for; matrix products, arithmetic and copies ran while one was open for 2% of the time, Pallas kernels for 48%

commit v1 on v0

--- a/solution.py
+++ b/solution.py
@@ -44,23 +44,32 @@
 
 
 def retention_kernel(
-    sp,
-    q_in, k_in, v_in, g_in, lam_ref,
-    q_home, k_home, v_home, k_head,
+    sp, dp,
+    q_in, k_in, v_in, g_in, x_in, w_in, lam_ref,
+    q_home, v_home, gi_out, dw_out,
     qa, ka, va, ga,
     qacc, kacc, vacc,
     dm0, dm1, dg0, dg1,
     sm0, sg1,
     run_a, run_b,
-    qh, kh, vh,
-    in_send, in_recv, out_send, out_recv, local_sem, head_sem,
+    qh, vh, kk, k_home, xa, wa, dw_send, dw_recv, dw_own, dw_sum,
+    in_send, in_recv, x_send, x_recv, out_send, out_recv, local_sem,
+    pair_send, pair_recv, w_send, w_recv, wf_send, wf_recv,
+    rs_send, rs_recv, ag_send, ag_recv, x_sem, w_sem, ag_sem,
 ):
     me = lax.axis_index("sp")
+    mine = lax.axis_index("dp")
+    side = lax.rem(me, 2)
+    partner = me + 1 - 2 * side
+    sibling = mine + 1 - 2 * lax.rem(mine, 2)
+    chips = dp // 2
+    half = xa.shape[2]
     dk = qa.shape[1]
     dv = va.shape[1]
     scaling = dk ** (-0.5)
     ins = ((q_in, qa, dk), (k_in, ka, dk), (v_in, va, dv), (g_in, ga, dv))
-    outs = ((qh, q_home, dk), (kh, k_home, dk), (vh, v_home, dv))
+    outs = ((qh, q_home, dk), (None, k_home, dk), (vh, v_home, dv))
+    my_side = pl.ds(pl.multiple_of(side * dk, dk), dk)
 
     def rows_of(b):
         return pl.ds(pl.multiple_of(b * BLOCK, BLOCK), BLOCK)
@@ -72,6 +81,14 @@
         pltpu.make_async_copy(src.at[:, cols_of(me, w)], dst.at[rows_of(me)], local_sem.at[t])
         for t, (src, dst, w) in enumerate(ins)
     ]
+    def x_cols(d, s):
+        return pl.ds(pl.multiple_of((2 * d + s) * half, half), half)
+
+    locals_x = [
+        pltpu.make_async_copy(x_in.at[:, x_cols(d, side)], xa.at[d, rows_of(me)], x_sem.at[d])
+        for d in range(dp)
+    ]
+    local_w = pltpu.make_async_copy(w_in, wa.at[mine], w_sem)
     for copy in locals_in:
         copy.start()
 
@@ -80,7 +97,11 @@
         pl.semaphore_signal(
             barrier, inc=1, device_id={"sp": lax.rem(me + off, sp)}, device_id_type=MESH
         )
-    pl.semaphore_wait(barrier, sp - 1)
+    for off in range(1, dp):
+        pl.semaphore_signal(
+            barrier, inc=1, device_id={"dp": lax.rem(mine + off, dp)}, device_id_type=MESH
+        )
+    pl.semaphore_wait(barrier, sp + dp - 2)
 
     def incoming(t, off):
         src, dst, w = ins[t]
@@ -97,6 +118,40 @@
     for off in range(1, sp):
         for t in range(4):
             incoming(t, off).start()
+
+    def weight(off):
+        return pltpu.make_async_remote_copy(
+            src_ref=w_in, dst_ref=wa.at[mine],
+            send_sem=w_send.at[off], recv_sem=w_recv.at[off],
+            device_id={"dp": lax.rem(mine + 2 * off, dp)}, device_id_type=MESH,
+        )
+
+    def weight_across(off):
+        owner = lax.rem(mine + dp - 2 * off, dp)
+        return pltpu.make_async_remote_copy(
+            src_ref=w_in if off == 0 else wa.at[owner], dst_ref=wa.at[owner],
+            send_sem=wf_send.at[off], recv_sem=wf_recv.at[off],
+            device_id={"dp": sibling}, device_id_type=MESH,
+        )
+
+    for off in range(1, chips):
+        weight(off).start()
+    weight_across(0).start()
+    local_w.start()
+
+    def rows_in(d, off):
+        peer = lax.rem(me + off, sp)
+        return pltpu.make_async_remote_copy(
+            src_ref=x_in.at[:, x_cols(d, lax.rem(peer, 2))], dst_ref=xa.at[d, rows_of(me)],
+            send_sem=x_send.at[d, off], recv_sem=x_recv.at[d, off],
+            device_id={"sp": peer}, device_id_type=MESH,
+        )
+
+    for copy in locals_x:
+        copy.start()
+    for off in range(1, sp):
+        for d in range(dp):
+            rows_in(d, off).start()
 
     def local_part(b):
         rows = rows_of(b)
@@ -143,13 +198,27 @@
 
     lax.fori_loop(0, sp, forward, 0)
 
+    for off in range(1, chips):
+        weight(off).wait_recv()
+        weight_across(off).start()
+
     run_a[...] = jnp.zeros_like(run_a)
     run_b[...] = jnp.zeros_like(run_b)
 
+    def held(t, b):
+        return kk.at[rows_of(b), my_side] if t == 1 else outs[t][0].at[rows_of(b)]
+
+    def paired(b):
+        return pltpu.make_async_remote_copy(
+            src_ref=kk.at[rows_of(b), my_side], dst_ref=kk.at[rows_of(b), my_side],
+            send_sem=pair_send.at[b], recv_sem=pair_recv.at[b],
+            device_id={"sp": partner}, device_id_type=MESH,
+        )
+
     def outgoing(t, b, source):
-        src, dst, w = outs[t]
-        return pltpu.make_async_remote_copy(
-            src_ref=src.at[rows_of(b)],
+        _, dst, w = outs[t]
+        return pltpu.make_async_remote_copy(
+            src_ref=held(t, b),
             dst_ref=dst.at[:, cols_of(source, w)],
             send_sem=out_send.at[t, b],
             recv_sem=out_recv.at[t, source],
@@ -158,8 +227,8 @@
         )
 
     def local_out(t):
-        src, dst, w = outs[t]
-        return pltpu.make_async_copy(src.at[rows_of(me)], dst.at[:, cols_of(me, w)], local_sem.at[t])
+        _, dst, w = outs[t]
+        return pltpu.make_async_copy(held(t, me), dst.at[:, cols_of(me, w)], local_sem.at[t])
 
     def backward(step, carry):
         b = sp - 1 - step
@@ -175,7 +244,9 @@
             + dot_nt(g, m0) * (jnp.exp(c0) * scaling)
             + dot_nt(g, m1) * (jnp.exp(c1) * scaling)
         ).astype(BF16)
-        kh[rows, :] = (kacc[rows, :] + dot_nt(v, g0) * ks0 + dot_nt(v, g1) * ks1).astype(BF16)
+        kk[rows, my_side] = (
+            kacc[rows, :] + dot_nt(v, g0) * ks0 + dot_nt(v, g1) * ks1
+        ).astype(BF16)
         vh[rows, :] = (
             vacc[rows, :]
             + dot_nn((kf * ks0).astype(BF16), g0)
@@ -184,6 +255,8 @@
         run_a[...] = jnp.exp(e0) * run_a[...] + dg0[b]
         run_b[...] = jnp.exp(e1) * run_b[...] + dm1[b]
 
+        paired(b).start()
+
         @pl.when(b != me)
         def _():
             for t in (1, 0, 2):
@@ -198,15 +271,62 @@
 
     lax.fori_loop(0, sp, backward, 0)
 
-    head_copy = pltpu.make_async_copy(kh, k_head, head_sem)
-    head_copy.start()
+    for copy in locals_x:
+        copy.wait()
+
+    def rows_arrived(off, carry):
+        for d in range(dp):
+            rows_in(d, off).wait_recv()
+        return carry
+
+    lax.fori_loop(1, sp, rows_arrived, 0)
+
+    def pair_arrived(b, carry):
+        paired(b).wait()
+        return carry
+
+    lax.fori_loop(0, sp, pair_arrived, 0)
+
+    def reducing(off):
+        peer = lax.rem(mine + off, dp)
+        return pltpu.make_async_remote_copy(
+            src_ref=dw_send.at[off], dst_ref=dw_recv.at[off],
+            send_sem=rs_send.at[off], recv_sem=rs_recv.at[off],
+            device_id={"dp": peer}, device_id_type=MESH,
+        )
+
+    for off in range(1, dp):
+        dw_send[off] = dot_tn(xa[lax.rem(mine + off, dp)], kk[...]).astype(BF16)
+    for off in range(1, dp):
+        reducing(off).start()
+    dw_own[...] = dot_tn(xa[mine], kk[...])
+    for off in range(1, dp):
+        reducing(off).wait_recv()
+        dw_own[...] += dw_recv[off].astype(F32)
+    dw_sum[...] = dw_own[...].astype(BF16)
+
+    def spot(device):
+        s = lax.rem(device, 2)
+        z = device // 2
+        return (
+            pl.ds(pl.multiple_of(s * half, half), half),
+            pl.ds(pl.multiple_of(z * (2 * dk), 2 * dk), 2 * dk),
+        )
+
+    def spreading(off):
+        return pltpu.make_async_remote_copy(
+            src_ref=dw_sum, dst_ref=dw_out.at[spot(me)],
+            send_sem=ag_send.at[off], recv_sem=ag_recv.at[off],
+            device_id={"sp": lax.rem(me + off, sp)}, device_id_type=MESH,
+        )
+
+    own_spot = pltpu.make_async_copy(dw_sum, dw_out.at[spot(me)], ag_sem)
+    own_spot.start()
+    for off in range(1, sp):
+        spreading(off).start()
 
     for t in range(3):
         local_out(t).wait()
-
-    for off in range(1, sp):
-        for t in range(4):
-            incoming(t, off).wait_send()
 
     def settle(off, carry):
         peer = lax.rem(me + off, sp)
@@ -215,26 +335,48 @@
         return carry
 
     lax.fori_loop(1, sp, settle, 0)
-    head_copy.wait()
-
-
-def retention_by_head(queries, key_vectors, values, cotangent, log_decay, sp):
-    tokens, hk = queries.shape
-    hv = values.shape[1]
+    local_w.wait()
+    for off in range(chips):
+        weight_across(off).wait()
+    rows_each = wa.shape[1]
+    for d in range(dp):
+        gi_out[:, d * rows_each : (d + 1) * rows_each] = dot_nt(k_home[...], wa[d]).astype(BF16)
+
+    for off in range(1, chips):
+        weight(off).wait_send()
+    for off in range(1, sp):
+        for t in range(4):
+            incoming(t, off).wait_send()
+        for d in range(dp):
+            rows_in(d, off).wait_send()
+    for off in range(1, dp):
+        reducing(off).wait_send()
+    own_spot.wait()
+    for off in range(1, sp):
+        spreading(off).wait()
+
+
+def shards_by_head(sp, dp, layer_input, queries, key_vectors, values, cotangent, log_decay, key_weight):
+    _, tokens, hk = queries.shape
+    hv = values.shape[2]
+    rows, width = key_weight.shape
     length = tokens * sp
     dk, dv = hk // HEADS, hv // HEADS
+    half = rows // 2
     lam = log_decay.reshape(2, sp, 1, BLOCK)
     anyspace = pl.BlockSpec(memory_space=pl.ANY)
-    return pl.pallas_call(
-        functools.partial(retention_kernel, sp),
+    vmem = pl.BlockSpec(memory_space=pltpu.VMEM)
+    dma = pltpu.SemaphoreType.DMA
+    grad_query, grad_value, grad_input, grad_weight = pl.pallas_call(
+        functools.partial(retention_kernel, sp, dp),
         out_shape=(
             jax.ShapeDtypeStruct((tokens, hk), BF16),
-            jax.ShapeDtypeStruct((tokens, hk), BF16),
             jax.ShapeDtypeStruct((tokens, hv), BF16),
-            jax.ShapeDtypeStruct((length, dk), BF16),
+            jax.ShapeDtypeStruct((tokens, rows * dp), BF16),
+            jax.ShapeDtypeStruct((rows, hk), BF16),
         ),
-        in_specs=[anyspace] * 4 + [pl.BlockSpec(memory_space=pltpu.VMEM)],
-        out_specs=(anyspace,) * 4,
+        in_specs=[anyspace] * 6 + [vmem],
+        out_specs=(anyspace, anyspace, vmem, anyspace),
         scratch_shapes=[
             pltpu.VMEM((length, dk), BF16),
             pltpu.VMEM((length, dk), BF16),
@@ -252,39 +394,25 @@
             pltpu.VMEM((dk, dv), F32),
             pltpu.VMEM((dk, dv), F32),
             pltpu.VMEM((length, dk), BF16),
-            pltpu.VMEM((length, dk), BF16),
             pltpu.VMEM((length, dv), BF16),
-            pltpu.SemaphoreType.DMA((4, sp)),
-            pltpu.SemaphoreType.DMA((4, sp)),
-            pltpu.SemaphoreType.DMA((3, sp)),
-            pltpu.SemaphoreType.DMA((3, sp)),
-            pltpu.SemaphoreType.DMA((4,)),
-            pltpu.SemaphoreType.DMA(()),
+            pltpu.VMEM((length, 2 * dk), BF16),
+            pltpu.VMEM((tokens, hk), BF16),
+            pltpu.VMEM((dp, length, half), BF16),
+            pltpu.VMEM((dp, rows, width), BF16),
+            pltpu.VMEM((dp, half, 2 * dk), BF16),
+            pltpu.VMEM((dp, half, 2 * dk), BF16),
+            pltpu.VMEM((half, 2 * dk), F32),
+            pltpu.VMEM((half, 2 * dk), BF16),
+            dma((4, sp)), dma((4, sp)), dma((dp, sp)), dma((dp, sp)),
+            dma((3, sp)), dma((3, sp)), dma((4,)),
+            dma((sp,)), dma((sp,)), dma((dp,)), dma((dp,)), dma((dp,)), dma((dp,)),
+            dma((dp,)), dma((dp,)), dma((sp,)), dma((sp,)), dma((dp,)), dma(()), dma(()),
         ],
         compiler_params=pltpu.CompilerParams(
-            collective_id=0, has_side_effects=True, vmem_limit_bytes=50 * 1024 * 1024
+            collective_id=0, has_side_effects=True, vmem_limit_bytes=60 * 1024 * 1024
         ),
-        cost_estimate=pl.CostEstimate(
-            flops=6_000_000_000, bytes_accessed=150_000_000, transcendentals=0
-        ),
-    )(queries, key_vectors, values, cotangent, lam)
-
-
-def shards_by_head(sp, layer_input, queries, key_vectors, values, cotangent, log_decay, key_weight):
-    all_weight = lax.all_gather(key_weight, "dp", axis=0, tiled=True)
-    all_rows = lax.all_gather(layer_input[0], "sp", axis=0, tiled=True)
-    grad_query, grad_key, grad_value, key_head = retention_by_head(
-        queries[0], key_vectors[0], values[0], cotangent[0], log_decay[0], sp
-    )
-    partial = lax.dot_general(
-        all_rows, key_head, (((0,), (0,)), ((), ())), preferred_element_type=F32
-    ).astype(BF16)
-    summed = lax.psum_scatter(partial, "dp", scatter_dimension=0, tiled=True)
-    grad_input = lax.dot_general(
-        grad_key, all_weight, (((1,), (1,)), ((), ())), preferred_element_type=F32
-    ).astype(BF16)
-    grad_weight = lax.all_gather(summed, "sp", axis=1, tiled=True).astype(F32)
-    return (grad_query[None], grad_value[None], grad_input[None], grad_weight)
+    )(queries[0], key_vectors[0], values[0], cotangent[0], layer_input[0], key_weight, lam)
+    return (grad_query[None], grad_value[None], grad_input[None], grad_weight.astype(F32))
 
 
 def unit_backward(query_rows, key_rows, value_rows, grad_rows, decay_rows, strict):
@@ -442,8 +570,9 @@
 
 def shards(*arrays):
     sp = lax.axis_size("sp")
-    if sp == HEADS and arrays[1].shape[1] == BLOCK:
-        return shards_by_head(sp, *arrays)
+    dp = lax.axis_size("dp")
+    if sp == HEADS and arrays[1].shape[1] == BLOCK and dp % 2 == 0:
+        return shards_by_head(sp, dp, *arrays)
     return shards_by_unit(*arrays)
 
 

time: 351 us -> 226 us (0.64); the launches traced: 347 us -> 226 us
  waiting for transfers between devices: 145 us -> 0 us
  Pallas kernels: 168 us -> 217 us
  between operations: 13.8 us -> 0.66 us
  matrix products: 11.5 us -> 0 us
  local copies, waits for them, and re-layouts: 8.64 us -> 3.88 us
  other arithmetic: 0 us -> 4.25 us
    all_gather x3 -> x0, waiting for transfers between devices: 103 us -> none  [the longest x1 60.4 us: shards_by_head(): all_weight = lax.all_gather(key_weight, 'dp', axis=0, tiled=True)]
    pallas_call x1, Pallas kernels: 168 us -> 217 us  [shards_by_head(): pl.pallas_call(functools.partial(retention_kernel, sp, dp), out_shape=(ja...]
    reduce_scatter x1 -> x0, waiting for transfers between devices: 40.8 us -> none  [shards_by_head(): summed = lax.psum_scatter(partial, 'dp', scatter_dimension=0, tiled=True)]
    dot_general x2 -> x0, matrix products: 11.5 us -> none  [the longest x1 7.06 us: shards_by_head(): lax.dot_general(grad_key, all_weight, (((1,), (1,)), ((), ())), preferred...]
    unnamed x7 -> x9, local copies, waits for them, and re-layouts: 7.92 us -> 2.57 us
    convert_element_type x0 -> x1, other arithmetic: none -> 4.25 us  [shards_by_head(): grad_weight.astype(F32)]
  transfers between devices with their start and end apart: 4 -> 0, of which waited for: 3 -> 0; matrix products, arithmetic and copies ran while one was open for 2% -> 0% of each run, Pallas kernels for 48% -> 0%
where the time goes in v1:
time: 226 us
  Pallas kernels  217 us (96%)
  other arithmetic  4.25 us (2%)
  local copies, waits for them, and re-layouts  3.88 us (2%)
    pallas_call x1, Pallas kernels, shards_by_head(): pl.pallas_call(functools.partial(retention_kernel, sp, dp), out_shape=(ja...  217 us

profile of v1, /device:TPU:15, one launch (start us, length us, event | category | flops | bytes accessed | tf_op | source)
XLA Modules:
  0.0 225.6 jit_solution(18347819920741498068)
XLA Ops:
  0.6 1.3 reshape.11.lam_ref
  1.9 216.8 %shard_map.102 = (bf16[128,2048]{1,0:T(8,128)(2,1)}, bf16[128,4096]{1,0:T(8,128)(2,1)}, bf16[128,2048]{1,0:T(8,128)(2,1)}, bf16[512,2048]{1,0:T(8,128)(2,1)}) custom-call(bf16[128,2048]{1,0:T(8,128)(2,1)} %bitcast.13, bf16[128,2048]{1,0:T(8,128)(2,1)} %bitcast.14, bf16[128,4096]{1,0:T(8,128)(2,1)} %bitcast.9, bf16[128,4096]{1,0:T(8,128)(2,1)} %bitcast.10, ...), custom_call_target="tpu_custom_call" | custom-call | tf_op jit(solution)/shard_map/pallas_call | solution.py:370
  218.7 0.0 copy-start.2
  218.7 0.0 copy-start
  218.7 4.2 %convert_element_type.3 = f32[512,2048]{1,0:T(8,128)} convert(bf16[512,2048]{1,0:T(8,128)(2,1)} %get-tuple-element.11) | non-fusion elementwise | flops 1048576 | bytes 6291456 | tf_op jit(solution)/shard_map/convert_element_type | solution.py:415
  223.0 0.0 copy-done.2
  223.0 0.0 copy-start.1
  223.0 0.8 copy.14
  223.8 0.0 copy-done
  223.8 1.0 copy.15
  224.8 0.0 copy-done.1
  224.8 0.8 copy.16
Async XLA Ops:
  218.7 4.3 %copy-start.2 = (bf16[128,2048]{1,0:T(8,128)(2,1)S(1)}, bf16[128,2048]{1,0:T(8,128)(2,1)}, u32[]{:S(2)}) copy-start(bf16[128,2048]{1,0:T(8,128)(2,1)} %get-tuple-element.8) | copy-start | bytes 1572868
  218.7 5.1 %copy-start = (bf16[128,4096]{1,0:T(8,128)(2,1)S(1)}, bf16[128,4096]{1,0:T(8,128)(2,1)}, u32[]{:S(2)}) copy-start(bf16[128,4096]{1,0:T(8,128)(2,1)} %get-tuple-element.9) | copy-start | bytes 3145732
  223.0 1.8 copy-start.1

commit v2 on v1

--- a/solution.py
+++ b/solution.py
@@ -56,6 +56,7 @@
     in_send, in_recv, x_send, x_recv, out_send, out_recv, local_sem,
     pair_send, pair_recv, w_send, w_recv, wf_send, wf_recv,
     rs_send, rs_recv, ag_send, ag_recv, x_sem, w_sem, ag_sem,
+    xf, xc_send, xc_recv, xg_send, xg_recv, af_send, af_recv,
 ):
     me = lax.axis_index("sp")
     mine = lax.axis_index("dp")
@@ -63,6 +64,13 @@
     partner = me + 1 - 2 * side
     sibling = mine + 1 - 2 * lax.rem(mine, 2)
     chips = dp // 2
+    group = sp // 2
+    first = (me // group) * group
+    far = lax.rem(me + group, sp)
+
+    def near(off):
+        return first + lax.rem(me - first + off, group)
+
     half = xa.shape[2]
     dk = qa.shape[1]
     dv = va.shape[1]
@@ -140,16 +148,34 @@
     local_w.start()
 
     def rows_in(d, off):
-        peer = lax.rem(me + off, sp)
+        peer = near(off) if off else far
         return pltpu.make_async_remote_copy(
             src_ref=x_in.at[:, x_cols(d, lax.rem(peer, 2))], dst_ref=xa.at[d, rows_of(me)],
             send_sem=x_send.at[d, off], recv_sem=x_recv.at[d, off],
             device_id={"sp": peer}, device_id_type=MESH,
         )
 
+    def rows_far(d):
+        return pltpu.make_async_remote_copy(
+            src_ref=x_in.at[:, x_cols(d, 1 - side)], dst_ref=xf.at[d],
+            send_sem=xc_send.at[d], recv_sem=xc_recv.at[d],
+            device_id={"sp": far}, device_id_type=MESH,
+        )
+
+    def rows_on(d, off):
+        return pltpu.make_async_remote_copy(
+            src_ref=xa.at[d, rows_of(far)] if off % 2 == 0 else xf.at[d],
+            dst_ref=xa.at[d, rows_of(far)],
+            send_sem=xg_send.at[d, off], recv_sem=xg_recv.at[d, off],
+            device_id={"sp": near(off)}, device_id_type=MESH,
+        )
+
     for copy in locals_x:
         copy.start()
-    for off in range(1, sp):
+    for d in range(dp):
+        rows_in(d, 0).start()
+        rows_far(d).start()
+    for off in range(1, group):
         for d in range(dp):
             rows_in(d, off).start()
 
@@ -259,13 +285,11 @@
 
         @pl.when(b != me)
         def _():
-            for t in (1, 0, 2):
-                outgoing(t, b, me).start()
+            outgoing(1, b, me).start()
 
         @pl.when(b == me)
         def _():
-            for t in range(3):
-                local_out(t).start()
+            local_out(1).start()
 
         return carry
 
@@ -274,12 +298,31 @@
     for copy in locals_x:
         copy.wait()
 
-    def rows_arrived(off, carry):
+    for d in range(dp):
+        rows_in(d, 0).wait_recv()
+        rows_far(d).wait_recv()
+    for off in range(1, group):
+        for d in range(dp):
+            rows_on(d, off).start()
+
+    for t in (0, 2):
+        local_out(t).start()
+
+    def send_rest(step, carry):
+        b = lax.rem(far + step, sp)
+        for t in (0, 2):
+            outgoing(t, b, me).start()
+        return carry
+
+    lax.fori_loop(0, group, send_rest, 0)
+    lax.fori_loop(group + 1, sp, send_rest, 0)
+
+    for off in range(1, group):
         for d in range(dp):
             rows_in(d, off).wait_recv()
-        return carry
-
-    lax.fori_loop(1, sp, rows_arrived, 0)
+    for off in range(1, group):
+        for d in range(dp):
+            rows_on(d, off).wait_recv()
 
     def pair_arrived(b, carry):
         paired(b).wait()
@@ -317,13 +360,23 @@
         return pltpu.make_async_remote_copy(
             src_ref=dw_sum, dst_ref=dw_out.at[spot(me)],
             send_sem=ag_send.at[off], recv_sem=ag_recv.at[off],
-            device_id={"sp": lax.rem(me + off, sp)}, device_id_type=MESH,
+            device_id={"sp": near(off) if off else far}, device_id_type=MESH,
+        )
+
+    def passing(off):
+        return pltpu.make_async_remote_copy(
+            src_ref=dw_out.at[spot(far)], dst_ref=dw_out.at[spot(far)],
+            send_sem=af_send.at[off], recv_sem=af_recv.at[off],
+            device_id={"sp": near(off)}, device_id_type=MESH,
         )
 
     own_spot = pltpu.make_async_copy(dw_sum, dw_out.at[spot(me)], ag_sem)
     own_spot.start()
-    for off in range(1, sp):
+    for off in range(group):
         spreading(off).start()
+    spreading(0).wait_recv()
+    for off in range(1, group):
+        passing(off).start()
 
     for t in range(3):
         local_out(t).wait()
@@ -347,13 +400,19 @@
     for off in range(1, sp):
         for t in range(4):
             incoming(t, off).wait_send()
-        for d in range(dp):
+    for d in range(dp):
+        rows_far(d).wait_send()
+        for off in range(group):
             rows_in(d, off).wait_send()
+        for off in range(1, group):
+            rows_on(d, off).wait_send()
     for off in range(1, dp):
         reducing(off).wait_send()
     own_spot.wait()
-    for off in range(1, sp):
+    spreading(0).wait_send()
+    for off in range(1, group):
         spreading(off).wait()
+        passing(off).wait()
 
 
 def shards_by_head(sp, dp, layer_input, queries, key_vectors, values, cotangent, log_decay, key_weight):
@@ -407,6 +466,8 @@
             dma((3, sp)), dma((3, sp)), dma((4,)),
             dma((sp,)), dma((sp,)), dma((dp,)), dma((dp,)), dma((dp,)), dma((dp,)),
             dma((dp,)), dma((dp,)), dma((sp,)), dma((sp,)), dma((dp,)), dma(()), dma(()),
+            pltpu.VMEM((dp, tokens, half), BF16),
+            dma((dp,)), dma((dp,)), dma((dp, sp)), dma((dp, sp)), dma((sp,)), dma((sp,)),
         ],
         compiler_params=pltpu.CompilerParams(
             collective_id=0, has_side_effects=True, vmem_limit_bytes=60 * 1024 * 1024
@@ -571,7 +632,7 @@
 def shards(*arrays):
     sp = lax.axis_size("sp")
     dp = lax.axis_size("dp")
-    if sp == HEADS and arrays[1].shape[1] == BLOCK and dp % 2 == 0:
+    if sp == HEADS and sp % 4 == 0 and arrays[1].shape[1] == BLOCK and dp % 2 == 0:
         return shards_by_head(sp, dp, *arrays)
     return shards_by_unit(*arrays)
 

time: 226 us -> 188 us (0.83)
  Pallas kernels: 217 us -> 178 us
    pallas_call x1, Pallas kernels: 217 us -> 178 us  [shards_by_head(): pl.pallas_call(functools.partial(retention_kernel, sp, dp), out_shape=(ja...]
where the time goes in v2:
time: 188 us; the launch traced here: 187 us
  Pallas kernels  178 us (95%)
  other arithmetic  4.25 us (2%)
  local copies, waits for them, and re-layouts  3.88 us (2%)
    pallas_call x1, Pallas kernels, shards_by_head(): pl.pallas_call(functools.partial(retention_kernel, sp, dp), out_shape=(ja...  178 us
    convert_element_type x1, other arithmetic, shards_by_head(): grad_weight.astype(F32)  4.25 us

profile of v2, /device:TPU:15, one launch (start us, length us, event | category | flops | bytes accessed | tf_op | source)
XLA Modules:
  0.0 186.6 jit_solution(3313770621327195817)
XLA Ops:
  0.6 1.3 reshape.11.lam_ref
  1.9 177.8 %shard_map.102 = (bf16[128,2048]{1,0:T(8,128)(2,1)}, bf16[128,4096]{1,0:T(8,128)(2,1)}, bf16[128,2048]{1,0:T(8,128)(2,1)}, bf16[512,2048]{1,0:T(8,128)(2,1)}) custom-call(bf16[128,2048]{1,0:T(8,128)(2,1)} %bitcast.13, bf16[128,2048]{1,0:T(8,128)(2,1)} %bitcast.14, bf16[128,4096]{1,0:T(8,128)(2,1)} %bitcast.9, bf16[128,4096]{1,0:T(8,128)(2,1)} %bitcast.10, ...), custom_call_target="tpu_custom_call" | custom-call | tf_op jit(solution)/shard_map/pallas_call | solution.py:429
  179.7 0.0 copy-start.2
  179.8 0.0 copy-start
  179.8 4.2 %convert_element_type.3 = f32[512,2048]{1,0:T(8,128)} convert(bf16[512,2048]{1,0:T(8,128)(2,1)} %get-tuple-element.11) | non-fusion elementwise | flops 1048576 | bytes 6291456 | tf_op jit(solution)/shard_map/convert_element_type | solution.py:476
  184.0 0.0 copy-done.2
  184.0 0.0 copy-start.1
  184.0 0.8 copy.14
  184.8 0.0 copy-done
  184.8 1.0 copy.15
  185.8 0.0 copy-done.1
  185.8 0.8 copy.16
Async XLA Ops:
  179.7 4.3 %copy-start.2 = (bf16[128,2048]{1,0:T(8,128)(2,1)S(1)}, bf16[128,2048]{1,0:T(8,128)(2,1)}, u32[]{:S(2)}) copy-start(bf16[128,2048]{1,0:T(8,128)(2,1)} %get-tuple-element.8) | copy-start | bytes 1572868
  179.8 5.1 %copy-start = (bf16[128,4096]{1,0:T(8,128)(2,1)S(1)}, bf16[128,4096]{1,0:T(8,128)(2,1)}, u32[]{:S(2)}) copy-start(bf16[128,4096]{1,0:T(8,128)(2,1)} %get-tuple-element.9) | copy-start | bytes 3145732
  184.0 1.8 copy-start.1
